TPU v7x, 128 devices: a whole 4x4x4 slice. The times are simulated.
128 devices in a mesh: sp: 64 (over z, y, x), tp: 2 (over core).
Axes of the slice: x: 4, y: 4, z: 4, core: 2. Of those that a mesh axis runs over, the one named last changes fastest.
Arguments:
- ssm_input: bfloat16 [16384, 1024], P('sp', 'tp'), may hold values from -6 to 6
- lam_real: float32 [64, 64], P('tp'), may hold values from -0.034 to -5.4931641e-06, as said below
- lam_imag: float32 [64, 64], P('tp'), may hold values from -3 to 3, as said below
- state_in: float32 [2, 64, 16, 64], P(None, 'tp'), may hold values from -2 to 2
- read_out: float32 [64, 128, 16], P('tp'), may hold values from -0.5 to 0.5
- channel_skip: float32 [1024], P('tp'), may hold values from -3 to 3
- glu_weight: bfloat16 [1024, 1024], replicated, may hold values from -0.1875 to 0.1875
- out_weight: bfloat16 [1024, 2048], replicated, may hold values from -0.375 to 0.375
- residual: bfloat16 [16384, 2048], P(('sp', 'tp')), may hold values from -6 to 6
- norm_gain: float32 [2048], replicated, may hold values from 0.1 to 1.9
- expert_ids: int32 [16384, 2], P(('sp', 'tp')), may hold values from 0 to 127, as said below
- route_weight: float32 [16384, 2], P(('sp', 'tp')), may hold values from 0.25 to 1
- expert_gate: bfloat16 [128, 2048, 512], P(('sp', 'tp')), may hold values from -0.125 to 0.125
- expert_up: bfloat16 [128, 2048, 512], P(('sp', 'tp')), may hold values from -0.125 to 0.125
- expert_down: bfloat16 [128, 512, 2048], P(('sp', 'tp')), may hold values from -0.25 to 0.25
Outputs:
- layer_out: bfloat16 [16384, 2048], P(('sp', 'tp'))
Inputs may be any that keep to these rules, and one draw needn't show every extreme that they name: `lam_real`: strictly negative. `lam_imag`: magnitude at least 0.5. `expert_ids`: A token's two experts differ and lie in the same group of 32 consecutive experts. Among the 128 rows of one device (aligned blocks) no expert is named more than 4 times, and some expert exactly 4 times; every expert is named in every such block.
All inputs are finite; a program needn't handle non-finite values.
Results may differ from a plain program's by a relative error of at most 0.006.
Values may be sent and summed in bfloat16 or wider, within the bound.
A program may use at most 128 MiB of HBM per device.

v0:
```python
import jax
import jax.numpy as jnp
from jax import lax
from jax.sharding import Mesh
from jax.sharding import PartitionSpec as P

GROUPS = 4
SP = ("sp_0", "sp_1", "sp_2")
SP_TP = ("sp_0", "sp_1", "sp_2", "tp")


EPSILON = 1e-06


def filled_with(array, identity):
    return jax.tree.map(
        lambda a, e: jnp.broadcast_to(jnp.asarray(e, a.dtype), a.shape), array, identity
    )


def collected_together(array, axis):
    leaves = jax.tree.leaves(array)
    order = sorted(range(len(leaves)), key=lambda k: -leaves[k].size)
    width = (1, *leaves[order[0]].shape)[-1]
    lines = [
        jnp.pad(leaves[k].reshape(-1), (0, -leaves[k].size % width)).reshape(-1, width)
        for k in order
    ]
    both, at, found = (lax.all_gather(jnp.concatenate(lines), axis), 0, {})
    for k, line in zip(order, lines):
        piece = both[:, at : at + len(line)].reshape(len(both), -1)
        found[k] = piece[:, : leaves[k].size].reshape(-1, *leaves[k].shape)
        at += len(line)
    numbers = iter(range(len(leaves)))
    return jax.tree.map(lambda _: found[next(numbers)], array)


def prefix_by_axis(array, axes, combine, identity):
    before = start = filled_with(array, identity)
    so_far = array
    for axis in reversed(axes):
        devices, mine = (lax.axis_size(axis), lax.axis_index(axis))
        pieces = collected_together(so_far, axis)
        inside, so_far = (start, start)
        for k in range(devices):
            passed = k < mine
            so_far = combine(so_far, jax.tree.map(lambda part: part[k], pieces))
            inside = jax.tree.map(lambda new, old: jnp.where(passed, new, old), so_far, inside)
        before = combine(inside, before)
    return before


def discretize(lam_real, lam_imag, state_in):
    magnitude = jnp.exp(lam_real)
    decay_re = magnitude * jnp.cos(lam_imag)
    decay_im = magnitude * jnp.sin(lam_imag)
    numer_re = decay_re - 1.0
    denom = lam_real * lam_real + lam_imag * lam_imag
    hold_re = ((numer_re * lam_real + decay_im * lam_imag) / denom)[:, None, :]
    hold_im = ((decay_im * lam_real - numer_re * lam_imag) / denom)[:, None, :]
    drive_re = hold_re * state_in[0] - hold_im * state_in[1]
    drive_im = hold_re * state_in[1] + hold_im * state_in[0]
    drive = jnp.concatenate([drive_re, drive_im], axis=-1).astype(jnp.bfloat16)
    return (decay_re, decay_im, drive)


def powers(lam_real, lam_imag, exponent):
    magnitude = jnp.exp(exponent[:, None, None] * lam_real[None])
    angle = exponent[:, None, None] * lam_imag[None]
    return (magnitude * jnp.cos(angle), magnitude * jnp.sin(angle))


def combine_steps(earlier, later):
    return (
        later[0] * earlier[0] - later[1] * earlier[1],
        later[0] * earlier[1] + later[1] * earlier[0],
        later[0] * earlier[2] - later[1] * earlier[3] + later[2],
        later[0] * earlier[3] + later[1] * earlier[2] + later[3],
    )


def block_states(push_re, push_im, decay_re, decay_im):
    shape_in = push_re.shape
    flat_re = push_re.reshape(shape_in[0], -1)
    flat_im = push_im.reshape(shape_in[0], -1)
    scale_re = jnp.broadcast_to(decay_re.reshape(1, -1), flat_re.shape)
    scale_im = jnp.broadcast_to(decay_im.reshape(1, -1), flat_im.shape)
    result = lax.associative_scan(combine_steps, (scale_re, scale_im, flat_re, flat_im), axis=0)
    return (result[2].reshape(shape_in), result[3].reshape(shape_in))


def readout(part_re, part_im, read_out):
    stacked = jnp.concatenate([part_re, part_im], axis=-1)
    return jnp.einsum("tgq,gqm->tgm", stacked, read_out, precision=lax.Precision.HIGHEST)


def run_expert(arrived, expert_gate, expert_up, expert_down):
    shape_in = arrived.shape
    flat_rows = arrived.reshape(-1, shape_in[-1])
    gate_part = jnp.dot(flat_rows, expert_gate[0], preferred_element_type=jnp.float32)
    up_part = jnp.dot(flat_rows, expert_up[0], preferred_element_type=jnp.float32)
    hidden = (jax.nn.silu(gate_part) * up_part).astype(jnp.bfloat16)
    answer = jnp.dot(hidden, expert_down[0], preferred_element_type=jnp.float32).astype(
        jnp.bfloat16
    )
    return answer.reshape(shape_in)


def on_device(
    ssm_input,
    lam_real,
    lam_imag,
    state_in,
    read_out,
    channel_skip,
    glu_weight,
    out_weight,
    residual,
    norm_gain,
    expert_ids,
    route_weight,
    expert_gate,
    expert_up,
    expert_down,
):
    token_rows = ssm_input.shape[0]
    group_count = lam_real.shape[0]
    state_size = lam_real.shape[1]
    channels = state_in.shape[2]
    decay_re, decay_im, drive = discretize(lam_real, lam_imag, state_in)
    inputs = ssm_input.reshape(token_rows, group_count, channels)
    pushed = jnp.einsum("tgm,gmp->tgp", inputs, drive, preferred_element_type=jnp.float32)
    push_re = pushed[..., :state_size]
    push_im = pushed[..., state_size:]
    span_re, span_im = powers(lam_real, lam_imag, jnp.full((1,), token_rows, jnp.float32))
    state_re, state_im = block_states(push_re, push_im, decay_re, decay_im)
    final_re = state_re[-1]
    final_im = state_im[-1]
    zeros_state = jnp.zeros_like(final_re)
    identity = (jnp.ones_like(final_re), zeros_state, zeros_state, zeros_state)
    incoming = prefix_by_axis(
        (span_re[0], span_im[0], final_re, final_im), SP, combine_steps, identity
    )
    in_re = incoming[2]
    in_im = incoming[3]
    ahead_re, ahead_im = powers(
        lam_real, lam_imag, jnp.arange(1, token_rows + 1).astype(jnp.float32)
    )
    carried_re = ahead_re * in_re - ahead_im * in_im
    carried_im = ahead_re * in_im + ahead_im * in_re
    read = readout(state_re, state_im, read_out) + readout(carried_re, carried_im, read_out)
    skips = channel_skip.reshape(group_count, channels)
    pre = jax.nn.gelu(read + skips * inputs.astype(jnp.float32)).astype(jnp.bfloat16)
    pre = pre.reshape(token_rows, group_count * channels)
    own_tokens = lax.all_to_all(pre, "tp", split_axis=0, concat_axis=1, tiled=True)
    gate_lin = jnp.dot(own_tokens, glu_weight, preferred_element_type=jnp.float32)
    gated = (own_tokens.astype(jnp.float32) * jax.nn.sigmoid(gate_lin)).astype(jnp.bfloat16)
    mixed = residual.astype(jnp.float32) + jnp.dot(
        gated, out_weight, preferred_element_type=jnp.float32
    )
    normed = (
        mixed * lax.rsqrt(jnp.mean(mixed * mixed, axis=-1, keepdims=True) + EPSILON) * norm_gain
    ).astype(jnp.bfloat16)
    token_count = normed.shape[0]
    model_width = normed.shape[1]
    route_count = expert_ids.shape[1]
    sp_count = lax.axis_size(SP)
    tp_count = lax.axis_size("tp")
    expert_count = sp_count * tp_count
    capacity = token_count * GROUPS // expert_count
    flat_ids = expert_ids.reshape(-1)
    onehot = (flat_ids[:, None] == jnp.arange(expert_count, dtype=jnp.int32)[None, :]).astype(
        jnp.int32
    )
    rank = jnp.sum(jnp.cumsum(onehot, axis=0) * onehot, axis=1) - 1
    position = flat_ids * capacity + rank
    slot_total = expert_count * capacity
    token_of = (
        jnp.zeros((slot_total,), jnp.int32)
        .at[position]
        .set(jnp.arange(token_count * route_count, dtype=jnp.int32) // route_count)
    )
    filled = jnp.zeros((slot_total,), jnp.bool_).at[position].set(True)
    outgoing = jnp.where(filled[:, None], normed[token_of], jnp.zeros((), jnp.bfloat16)).reshape(
        expert_count, capacity, model_width
    )
    answered = run_expert(
        lax.all_to_all(outgoing, SP_TP, split_axis=0, concat_axis=0, tiled=True),
        expert_gate,
        expert_up,
        expert_down,
    )
    returned = lax.all_to_all(answered, SP_TP, split_axis=0, concat_axis=0, tiled=True)
    answers = returned.reshape(slot_total, model_width)[position].astype(jnp.float32)
    answers = answers.reshape(token_count, route_count, model_width)
    routed = jnp.sum(answers * route_weight[:, :, None], axis=1)
    return (mixed + routed).astype(jnp.bfloat16)


def solution(mesh):
    torus = Mesh(mesh.devices.reshape(4, 4, 4, mesh.shape["tp"]), ("sp_0", "sp_1", "sp_2", "tp"))
    in_specs = (
        P(SP, "tp"),
        P("tp", None),
        P("tp", None),
        P(None, "tp", None, None),
        P("tp", None, None),
        P("tp"),
        P(),
        P(),
        P(SP_TP, None),
        P(),
        P(SP_TP, None),
        P(SP_TP, None),
        P(SP_TP, None, None),
        P(SP_TP, None, None),
        P(SP_TP, None, None),
    )
    out_specs = P(SP_TP, None)
    return jax.shard_map(
        on_device, mesh=torus, in_specs=in_specs, out_specs=out_specs, check_vma=False
    )
```

profile of v0, /device:TPU:1, one launch (start us, length us, event | category | flops | bytes accessed | tf_op | source)
XLA Modules:
  0.0 621.4 jit_solution(1390810379706939283)
XLA Ops:
  9.0 39.8 %slice.587 = f32[128,2048]{0,1:T(8,128)} slice(f32[256,2048]{0,1:T(8,128)} %bitcast.434), slice={[1:256:2], [0:2048:1]} | slice | bytes 2097152 | tf_op jit(solution)/shard_map/slice | solution.py:88
  48.7 39.4 %slice.580 = f32[128,2048]{0,1:T(8,128)S(1)} slice(f32[256,2048]{0,1:T(8,128)} %bitcast.435), slice={[0:255:2], [0:2048:1]} | slice | bytes 2097152 | tf_op jit(solution)/shard_map/slice | solution.py:88
  88.1 39.5 %slice.675 = f32[127,2048]{0,1:T(8,128)} slice(f32[256,2048]{0,1:T(8,128)} %bitcast.436), slice={[2:256:2], [0:2048:1]} | slice | bytes 2080768 | tf_op jit(solution)/shard_map/slice | solution.py:88
  127.6 39.8 %slice.581 = f32[128,2048]{0,1:T(8,128)} slice(f32[256,2048]{0,1:T(8,128)} %bitcast.431), slice={[1:256:2], [0:2048:1]} | slice | bytes 2097152 | tf_op jit(solution)/shard_map/slice | solution.py:88
  167.4 39.9 %slice.577 = f32[128,2048]{0,1:T(8,128)} slice(f32[256,2048]{0,1:T(8,128)} %bitcast.432), slice={[0:255:2], [0:2048:1]} | slice | bytes 2097152 | tf_op jit(solution)/shard_map/slice | solution.py:88
  207.4 39.5 %slice.672 = f32[127,2048]{0,1:T(8,128)} slice(f32[256,2048]{0,1:T(8,128)} %bitcast.433), slice={[2:256:2], [0:2048:1]} | slice | bytes 2080768 | tf_op jit(solution)/shard_map/slice | solution.py:88
  343.0 4.6 pad.124
  347.6 4.7 pad.123
  352.3 4.7 pad.125
  364.8 8.6 %pad.126 = f32[256,2048]{1,0:T(8,128)} pad(f32[128,2048]{1,0:T(8,128)} %pad_maximum_fusion, f32[]{:T(128)} %constant.24.clone.1), padding=0_1_1x0_0_0 | pad | bytes 3145732 | tf_op jit(solution)/shard_map/pad | solution.py:88
  373.4 4.8 pad.127
  379.1 4.0 add.875
  384.3 8.7 %pad.128 = f32[256,2048]{1,0:T(8,128)} pad(f32[128,2048]{1,0:T(8,128)} %pad_maximum_fusion.1, f32[]{:T(128)} %constant.24.clone.1), padding=0_1_1x0_0_0 | pad | bytes 3145732 | tf_op jit(solution)/shard_map/pad | solution.py:88
  393.0 4.8 pad.129
  408.8 11.0 %all-gather = f32[512,64]{1,0:T(8,128)S(1)} all-gather(f32[128,64]{1,0:T(8,128)S(1)} %pad_maximum_fusion.10), channel_id=2, replica_groups=mesh['sp_0'=4,'sp_1'=4,'sp_2'=4,'tp'=2] {'sp_2'}, dimensions={0}, use_global_device_ids=true | all-gather | bytes 163840 | tf_op jit(solution)/shard_map/all_gather | solution.py:29
  419.9 9.9 %all-gather.1 = f32[512,64]{1,0:T(8,128)S(1)} all-gather(f32[128,64]{1,0:T(8,128)S(1)} %pad_maximum_fusion.11), channel_id=3, replica_groups=mesh['sp_0'=4,'sp_1'=4,'sp_2'=4,'tp'=2] {'sp_1'}, dimensions={0}, use_global_device_ids=true | all-gather | bytes 163840 | tf_op jit(solution)/shard_map/all_gather | solution.py:29
  429.9 11.3 %all-gather.2 = f32[512,64]{1,0:T(8,128)} all-gather(f32[128,64]{1,0:T(8,128)S(1)} %pad_maximum_fusion.12), channel_id=4, replica_groups=mesh['sp_0'=4,'sp_1'=4,'sp_2'=4,'tp'=2] {'sp_0'}, dimensions={0}, use_global_device_ids=true | all-gather | bytes 163840 | tf_op jit(solution)/shard_map/all_gather | solution.py:29
  448.9 7.7 %fusion.2 = f32[32,256,16]{1,2,0:T(8,128)S(1)} fusion(f32[32,128,16]{1,2,0:T(8,128)} %param.19, f32[256,32,64]{2,0,1:T(8,128)} %copy.53, f32[256,32,64]{2,0,1:T(8,128)} %copy.52), kind=kOutput, calls=%fused_computation.8 | convolution fusion | flops 202375168 | bytes 4980736 | tf_op jit(solution)/shard_map/tgq,gqm->tgm/dot_general | solution.py:94
  456.8 16.5 %multiply_subtract_fusion = (f32[256,32,64]{2,0,1:T(8,128)S(1)}, f32[256,32,64]{2,0,1:T(8,128)S(1)}) fusion(f32[32,64]{1,0:T(8,128)S(1)} %add_bitcast_fusion, f32[32,64]{1,0:T(8,128)S(1)} %get-tuple-element.7, f32[32,64]{1,0:T(8,128)S(1)} %copy-done.39, f32[32,64]{1,0:T(8,128)S(1)} %copy-done.40, f32[256]{0:T(256)S(1)} %copy-done.61), kind=kLoop, calls=%fused_computation.17 | loop fusion | flops 5242880 | bytes 4228096 | tf_op jit(solution)/shard_map/sub | solution.py:149
  473.3 4.3 fusion.46
  478.4 12.3 %all-to-all-start = ((bf16[2,128,512]{1,2,0:T(8,128)(2,1)}), bf16[2,128,512]{1,2,0:T(8,128)(2,1)S(1)}, u32[]{:S(2)}, u32[]{:S(2)}) async-start(bf16[2,128,512]{1,2,0:T(8,128)(2,1)} %copy.54), calls=%async_computation | async-start | bytes 524288 | tf_op jit(solution)/shard_map/all_to_all | solution.py:155
  495.3 5.0 multiply_reduce_fusion.1
  505.0 4.1 gather.9
  511.7 38.3 %all_to_all.29 = bf16[128,4,2048]{2,1,0:T(4,128)(2,1)} all-to-all(bf16[128,4,2048]{2,1,0:T(4,128)(2,1)S(1)} %broadcast_select_fusion), channel_id=1, replica_groups=mesh['sp_0'=4,'sp_1'=4,'sp_2'=4,'tp'=2] {'sp_0','sp_1','sp_2','tp'}, dimensions={0} | all-to-all | bytes 4194304 | tf_op jit(solution)/shard_map/all_to_all | solution.py:188
  550.0 4.0 reshape.299
  554.0 4.5 fusion.13
  558.4 6.3 %convolution_convert_fusion = bf16[512,2048]{1,0:T(8,128)(2,1)} fusion(bf16[1,512,2048]{2,1,0:T(8,128)(2,1)S(1)} %copy-done, bf16[512,2048]{1,0:T(8,128)(2,1)} %reshape.299, bf16[1,2048,512]{2,1,0:T(8,128)(2,1)} %param.28, f32[512,512]{1,0:T(8,128)} %fusion.13), kind=kOutput, calls=%fused_computation.19 | convolution fusion | flops 2150105088 | bytes 9437184 | tf_op jit(solution)/shard_map/dot_general | solution.py:103
  564.7 4.1 reshape.300
  568.8 5.6 all-to-all-start.2
  574.5 30.1 %all-to-all-done.2 = bf16[128,4,2048]{2,1,0:T(4,128)(2,1)} async-done(((bf16[128,4,2048]{2,1,0:T(4,128)(2,1)}), bf16[128,4,2048]{2,1,0:T(4,128)(2,1)}, u32[]{:S(2)}, u32[]{:S(2)}) %all-to-all-start.2) | async-done | bytes 2097184 | tf_op jit(solution)/shard_map/all_to_all | solution.py:193
  608.6 4.2 gather_fusion.1
  615.2 4.9 multiply_reduce_fusion
  (314 shorter events, 153.2 us)
Async XLA Ops:
  0.0 558.4 %copy-start = (bf16[1,512,2048]{2,1,0:T(8,128)(2,1)S(1)}, bf16[1,512,2048]{2,1,0:T(8,128)(2,1)}, u32[]{:S(2)}) copy-start(bf16[1,512,2048]{2,1,0:T(8,128)(2,1)} %param.29) | copy-start | bytes 6291460
  246.9 8.6 %copy-start.25 = (f32[2048]{0:T(1024)}, f32[2048]{0:T(1024)S(1)}, u32[]{:S(2)}) copy-start(f32[2048]{0:T(1024)S(1)} %broadcast_in_dim.25) | copy-start | bytes 24580
  247.0 8.5 %copy-start.27 = (f32[2048]{0:T(1024)}, f32[2048]{0:T(1024)S(1)}, u32[]{:S(2)}) copy-start(f32[2048]{0:T(1024)S(1)} %broadcast_in_dim.24) | copy-start | bytes 24580
  255.5 19.1 %copy-start.29 = (f32[2048]{0:T(1024)}, f32[2048]{0:T(1024)S(1)}, u32[]{:S(2)}) copy-start(f32[2048]{0:T(1024)S(1)} %get-tuple-element.39) | copy-start | bytes 24580
  255.5 19.1 %copy-start.31 = (f32[2048]{0:T(1024)}, f32[2048]{0:T(1024)S(1)}, u32[]{:S(2)}) copy-start(f32[2048]{0:T(1024)S(1)} %get-tuple-element.40) | copy-start | bytes 24580
  255.5 25.5 %copy-start.33 = (f32[2048]{0:T(1024)}, f32[2048]{0:T(1024)S(1)}, u32[]{:S(2)}) copy-start(f32[2048]{0:T(1024)S(1)} %get-tuple-element.37) | copy-start | bytes 24580
  255.5 25.5 %copy-start.35 = (f32[2048]{0:T(1024)}, f32[2048]{0:T(1024)S(1)}, u32[]{:S(2)}) copy-start(f32[2048]{0:T(1024)S(1)} %get-tuple-element.38) | copy-start | bytes 24580
  285.5 28.6 %copy-start.9 = (f32[127,2048]{0,1:T(8,128)S(1)}, f32[127,2048]{0,1:T(8,128)}, u32[]{:S(2)}) copy-start(f32[127,2048]{0,1:T(8,128)} %slice.675) | copy-start | bytes 3121156
  314.1 4.5 copy-start.24
  330.4 6.6 %copy-start.30 = (f32[2048]{0:T(1024)S(1)}, f32[2048]{0:T(1024)}, u32[]{:S(2)}) copy-start(f32[2048]{0:T(1024)} %copy-done.29) | copy-start | bytes 24580
  330.4 6.6 %copy-start.32 = (f32[2048]{0:T(1024)S(1)}, f32[2048]{0:T(1024)}, u32[]{:S(2)}) copy-start(f32[2048]{0:T(1024)} %copy-done.31) | copy-start | bytes 24580
  333.1 4.0 copy-start.5
  333.1 4.0 copy-start.6
  333.1 4.0 copy-start.15
  333.1 4.0 copy-start.16
  364.8 8.6 %copy-start.8 = (f32[128,2048]{1,0:T(8,128)S(1)}, f32[128,2048]{1,0:T(8,128)}, u32[]{:S(2)}) copy-start(f32[128,2048]{1,0:T(8,128)} %add.870) | copy-start | bytes 3145732
  379.1 4.0 copy-start.41
  379.1 4.1 copy-start.14
  384.3 8.7 %copy-start.7 = (f32[128,2048]{1,0:T(8,128)S(1)}, f32[128,2048]{1,0:T(8,128)}, u32[]{:S(2)}) copy-start(f32[128,2048]{1,0:T(8,128)} %add.873) | copy-start | bytes 3145732
  398.8 4.0 copy-start.59
  448.9 7.7 %copy-start.18 = (f32[512,64]{1,0:T(8,128)S(1)}, f32[512,64]{1,0:T(8,128)}, u32[]{:S(2)}) copy-start(f32[512,64]{1,0:T(8,128)} %all-gather.2) | copy-start | bytes 393220
  448.9 7.9 %copy-start.39 = (f32[32,64]{1,0:T(8,128)S(1)}, f32[32,64]{1,0:T(8,128)}, u32[]{:S(2)}) copy-start(f32[32,64]{1,0:T(8,128)} %param.17) | copy-start | bytes 24580
  448.9 7.9 %copy-start.40 = (f32[32,64]{1,0:T(8,128)S(1)}, f32[32,64]{1,0:T(8,128)}, u32[]{:S(2)}) copy-start(f32[32,64]{1,0:T(8,128)} %param.16) | copy-start | bytes 24580
  448.9 7.9 %copy-start.61 = (f32[256]{0:T(256)S(1)}, f32[256]{0:T(256)}, u32[]{:S(2)}) copy-start(f32[256]{0:T(256)} %add_convert_fusion.1) | copy-start | bytes 3076
  456.8 16.5 %copy-start.17 = (f32[32,128,16]{1,2,0:T(8,128)S(1)}, f32[32,128,16]{1,2,0:T(8,128)}, u32[]{:S(2)}) copy-start(f32[32,128,16]{1,2,0:T(8,128)} %param.19) | copy-start | bytes 786436
  473.3 17.5 %copy-start.58 = (s32[128,2]{0,1:T(2,128)S(1)}, s32[128,2]{0,1:T(2,128)}, u32[]{:S(2)}) copy-start(s32[128,2]{0,1:T(2,128)} %param.25) | copy-start | bytes 3076
  477.6 17.7 %copy-start.62 = (bf16[128,2048]{1,0:T(8,128)(2,1)S(1)}, bf16[128,2048]{1,0:T(8,128)(2,1)}, u32[]{:S(2)}) copy-start(bf16[128,2048]{1,0:T(8,128)(2,1)} %param.23) | copy-start | bytes 1572868
  478.4 16.7 %all-to-all-start = ((bf16[2,128,512]{1,2,0:T(8,128)(2,1)}), bf16[2,128,512]{1,2,0:T(8,128)(2,1)S(1)}, u32[]{:S(2)}, u32[]{:S(2)}) async-start(bf16[2,128,512]{1,2,0:T(8,128)(2,1)} %copy.54), calls=%async_computation | async-start | bytes 524288 | tf_op jit(solution)/shard_map/all_to_all | solution.py:155
  495.3 5.0 copy-start.57
  568.8 5.6 copy-start.60
  568.8 35.8 %all-to-all-start.2 = ((bf16[128,4,2048]{2,1,0:T(4,128)(2,1)}), bf16[128,4,2048]{2,1,0:T(4,128)(2,1)}, u32[]{:S(2)}, u32[]{:S(2)}) async-start(bf16[128,4,2048]{2,1,0:T(4,128)(2,1)} %reshape.300), calls=%async_computation.2 | async-start | bytes 4194304 | tf_op jit(solution)/shard_map/all_to_all | solution.py:193
  615.2 4.9 copy-start.10
  (33 other events, 88.4 us)
where the time goes:
time: 634 us; the launch traced here: 621 us
  local copies, waits for them, and re-layouts  398 us (63%)
  other arithmetic  74.7 us (12%)
  blocking collectives  70.4 us (11%)
  waiting for transfers between devices  30.1 us (5%)
  matrix products  28.8 us (5%)
  starting transfers between devices  17.9 us (3%)
    slice x53, local copies, waits for them, and re-layouts, block_states(): lax.associative_scan(combine_steps, (scale_re, scale_im, flat_re, flat_im...  283 us
    pad x28, local copies, waits for them, and re-layouts, block_states(): lax.associative_scan(combine_steps, (scale_re, scale_im, flat_re, flat_im...  49.8 us
    all_to_all x1, blocking collectives, on_device(): lax.all_to_all(outgoing, SP_TP, split_axis=0, concat_axis=0, tiled=True)  38.3 us
    all_gather x3, blocking collectives, collected_together(): both, at, found = (lax.all_gather(jnp.concatenate(lines), axis), 0, {})  32.2 us
    all_to_all x1, waiting for transfers between devices, on_device(): lax.all_to_all(answered, SP_TP, split_axis=0, concat_axis=0, tiled=True)  30.1 us
    add x17, other arithmetic, block_states(): lax.associative_scan(combine_steps, (scale_re, scale_im, flat_re, flat_im...  19.2 us
    sub x1, other arithmetic, on_device(): carried_re = ahead_re * in_re - ahead_im * in_im  16.5 us
    unnamed x136, local copies, waits for them, and re-layouts  16.5 us
  transfers between devices with their start and end apart: 2, of which 1 were waited for; matrix products, arithmetic and copies ran while one was open for 1% of the time, Pallas kernels for 0%

commit v1 on v0

v1 whole, which is shorter than its diff:
```python
import functools

import jax
import jax.numpy as jnp
from jax import lax
from jax.experimental import pallas as pl
from jax.experimental.pallas import tpu as pltpu
from jax.sharding import PartitionSpec as P

EPSILON = 1e-06
F32 = jnp.float32
BF16 = jnp.bfloat16
MESH = pl.DeviceIdType.MESH
SEG = 8
STEPS = 32
CHUNKS = 4
PER_CHUNK = 16


def dot(a, b):
    return jnp.dot(a, b, preferred_element_type=F32)


def iota(shape, dim):
    return lax.broadcasted_iota(jnp.int32, shape, dim)


def complex_mul(a, b):
    return a[0] * b[0] - a[1] * b[1], a[0] * b[1] + a[1] * b[0]


def complex_fma(a, b, c):
    return a[0] * b[0] - a[1] * b[1] + c[0], a[0] * b[1] + a[1] * b[0] + c[1]


def power(lam_real, lam_imag, exponent):
    magnitude = jnp.exp(exponent * lam_real)
    angle = exponent * lam_imag
    turns = jnp.floor(angle * 0.15915494309189535 + 0.5)
    angle = (angle - turns * 6.28125) - turns * 0.0019353071795864769
    return magnitude * jnp.cos(angle), magnitude * jnp.sin(angle)


def lanes_of(rows):
    return jnp.concatenate([rows[i : i + 1, :] for i in range(rows.shape[0])], axis=1)


def body(
    u_ref, lr_ref, li_ref, in_ref, ro_ref, skip_ref, gain_ref, meta_ref,
    glu_hbm, outw_hbm, res_hbm, wg_hbm, wu_hbm, wd_hbm,
    o_ref,
    glu, outw, res, wg, wu, wd, meta2,
    push, edge, fin, xbuf, ybuf, line, st, cblk, hot, comb,
    pre, mixed, normed, send, recv, ans, ret, part_out, part_in,
    hsem, xs, xr, ys, yr, psend, precv, ssem, rsem, asem, bsem,
):
    c = lax.axis_index("sp")
    k = lax.axis_index("tp")
    other = 1 - k
    z, y, x = c // 16, (c // 4) % 4, c % 4
    ln = c // 4

    def chip_at(i, sign):
        dz, dy, dx = i // 16, (i // 4) % 4, i % 4
        return (
            ((z + sign * dz + 4) % 4) * 16 + ((y + sign * dy + 4) % 4) * 4 + (x + sign * dx + 4) % 4
        )

    loads = [
        pltpu.make_async_copy(glu_hbm, glu, hsem.at[0]),
        pltpu.make_async_copy(outw_hbm, outw, hsem.at[1]),
        pltpu.make_async_copy(res_hbm, res.at[k], hsem.at[2]),
        pltpu.make_async_copy(wg_hbm.at[0], wg, hsem.at[3]),
        pltpu.make_async_copy(wu_hbm.at[0], wu, hsem.at[4]),
        pltpu.make_async_copy(wd_hbm.at[0], wd, hsem.at[5]),
    ]
    for load in loads:
        load.start()

    barrier = pltpu.get_barrier_semaphore()
    pl.semaphore_signal(barrier, inc=1, device_id=(c, other), device_id_type=MESH)

    def greet(i, carry):
        pl.semaphore_signal(barrier, inc=1, device_id=(chip_at(i, 1), k), device_id_type=MESH)
        return carry

    lax.fori_loop(1, 64, greet, 0)

    lam_r, lam_i = lr_ref[...], li_ref[...]
    decay_re, decay_im = power(lam_r, lam_i, 1.0)
    numer_re = decay_re - 1.0
    denom = lam_r * lam_r + lam_i * lam_i
    hold_re = (numer_re * lam_r + decay_im * lam_i) / denom
    hold_im = (decay_im * lam_r - numer_re * lam_i) / denom
    hold_re = jnp.broadcast_to(hold_re[:, None, :], (32, 16, 64)).reshape(512, 64)
    hold_im = jnp.broadcast_to(hold_im[:, None, :], (32, 16, 64)).reshape(512, 64)
    drive = (
        (hold_re * in_ref[0] - hold_im * in_ref[1]).astype(BF16),
        (hold_re * in_ref[1] + hold_im * in_ref[0]).astype(BF16),
    )
    spread = (iota((64, 1024), 1) % 64 == iota((64, 1024), 0)).astype(F32).astype(BF16)
    own_block = iota((256, 1024), 0) // 16 == iota((256, 1024), 1) // 64
    row, col = iota((256, 256), 0), iota((256, 256), 1)
    order = (col == (row % SEG) * STEPS + row // SEG).astype(F32).astype(BF16)
    unorder = (row == (col % SEG) * STEPS + col // SEG).astype(F32).astype(BF16)
    ordered = dot(order, u_ref[...]).astype(BF16)
    for half in range(2):
        for part in range(2):
            block = dot(drive[part][256 * half : 256 * half + 256], spread)
            block = jnp.where(own_block, block, 0.0).astype(BF16)
            push[part, :, 1024 * half : 1024 * half + 1024] = dot(
                ordered[:, 256 * half : 256 * half + 256], block
            )

    dense_r, dense_i = meta_ref[8:24, :], meta_ref[24:40, :]
    p1 = power(dense_r, dense_i, 1.0)
    p32 = power(dense_r, dense_i, 32.0)
    p64 = power(dense_r, dense_i, 64.0)
    p128 = power(dense_r, dense_i, 128.0)
    q1 = power(dense_r, dense_i, 256.0)
    q2 = complex_mul(q1, q1)
    q3 = complex_mul(q2, q1)
    q4 = complex_mul(q2, q2)
    one = (jnp.ones_like(dense_r), jnp.zeros_like(dense_r))

    def segment_powers(j):
        def lane(v):
            return jnp.broadcast_to(lanes_of(v[4 * j : 4 * j + 4, :]), (8, 512))

        return [tuple(lane(v) for v in p) for p in (p1, p32, p64, p128)]

    seg = iota((8, 512), 0)
    for j in range(4):
        at = 512 * j
        d1, d32, d64, d128 = segment_powers(j)

        def step(i, h):
            rows = pl.ds(pl.multiple_of(i * 8, 8), 8)
            return complex_fma(d1, h, (push[0, rows, at : at + 512], push[1, rows, at : at + 512]))

        zero = jnp.zeros((8, 512), F32)
        h = lax.fori_loop(0, STEPS, step, (zero, zero), unroll=4)
        for d, p in ((1, d32), (2, d64), (4, d128)):
            moved = tuple(jnp.where(seg >= d, pltpu.roll(v, d, 0), 0.0) for v in h)
            h = complex_fma(p, moved, h)
        for part in range(2):
            edge[part, :, at : at + 512] = jnp.where(seg >= 1, pltpu.roll(h[part], 1, 0), 0.0)
            for n in range(4):
                fin[part, 4 * j + n : 4 * j + n + 1, :] = h[part][7:8, 128 * n : 128 * n + 128]

    pl.semaphore_wait(barrier, 64)

    def remote(src, dst, s, r, device):
        return pltpu.make_async_remote_copy(
            src_ref=src, dst_ref=dst, send_sem=s, recv_sem=r, device_id=device, device_id_type=MESH
        )

    along = [
        remote(fin, xbuf.at[d - 1], xs.at[d - 1], xr.at[d - 1], (c - x + (x + d) % 4, k))
        for d in (1, 2, 3)
    ]
    for copy in along:
        copy.start()
    meta_copy = remote(meta_ref.at[0:8], meta2, psend.at[0], precv.at[0], (c, other))
    meta_copy.start()
    res_copy = remote(res_hbm, res.at[k], psend.at[1], precv.at[1], (c, other))
    res_copy.start()

    narrow = (iota((16, 256), 1) % 16 == iota((16, 256), 0)).astype(F32).astype(BF16)
    own_read = iota((1024, 256), 0) // 64 == iota((1024, 256), 1) // 16
    for half in range(2):
        for part in range(2):
            piece = ro_ref[16 * half : 16 * half + 16, 64 * part : 64 * part + 64, :]
            piece = dot(piece.reshape(1024, 16).astype(BF16), narrow)
            cblk[half, 1024 * part : 1024 * part + 1024, :] = jnp.where(own_read, piece, 0.0).astype(BF16)

    for copy in along:
        copy.wait()

    def pick(n):
        return tuple(
            jnp.where(n == 0, a, jnp.where(n == 1, b, jnp.where(n == 2, e, f)))
            for a, b, e, f in zip(one, q1, q2, q3)
        )

    own = (fin[0], fin[1])
    total = complex_mul(pick(3 - x), own)
    inside = (jnp.zeros_like(dense_r), jnp.zeros_like(dense_r))
    for d in (1, 2, 3):
        theirs = (xbuf[d - 1, 0], xbuf[d - 1, 1])
        total = complex_fma(pick(3 - (x - d + 4) % 4), theirs, total)
        grown = complex_fma((one, q1, q2)[d - 1], theirs, inside)
        inside = tuple(jnp.where(d <= x, a, b) for a, b in zip(grown, inside))
    line[0] = total[0]
    line[1] = total[1]

    def to_line(target, carry):
        remote(line, ybuf.at[ln], ys.at[target], yr.at[ln], (target * 4 + x, k)).start()
        return carry

    lax.fori_loop(ln + 1, 16, to_line, 0)

    meta_copy.wait()
    slot = iota((64, 128), 0)
    chip = (
        ((z + slot // 16) % 4) * 16 + ((y + (slot // 4) % 4) % 4) * 4 + (x + slot % 4) % 4
    )
    expert = (chip * 2 + k).astype(F32)
    before = (iota((128, 128), 0) < iota((128, 128), 1)).astype(F32).astype(BF16)
    sub = iota((64, 8, 128), 1)
    own_meta, other_meta = meta_ref[0:8, :], meta2[...]
    for b in range(2):
        m = jnp.where(k == b, own_meta, other_meta)
        first = m[0:1, :] == expert
        second = m[1:2, :] == expert
        named = jnp.logical_or(first, second)
        rank = dot(named.astype(F32).astype(BF16), before)
        rank = jnp.where(named, rank + 4.0 * b, -1.0)
        weight = jnp.where(first, m[2:3, :], m[3:4, :])
        hit = rank[:, None, :] == sub.astype(F32)
        hot[:, 128 * b : 128 * b + 128] = hit.astype(F32).reshape(512, 128).astype(BF16)
        scaled = jnp.where(hit, weight[:, None, :], 0.0).reshape(512, 128)
        scaled = scaled.T
        high = scaled.astype(BF16)
        comb[b, :, 0:512] = high
        comb[b, :, 512:1024] = (scaled - high.astype(F32)).astype(BF16)

    def from_line(n, acc):
        remote(line, ybuf.at[n], ys.at[0], yr.at[n], (c, other)).wait_recv()
        return complex_fma(q4, acc, (ybuf[n, 0], ybuf[n, 1]))

    earlier = lax.fori_loop(0, ln, from_line, (jnp.zeros_like(dense_r), jnp.zeros_like(dense_r)))
    incoming = complex_fma(pick(x), earlier, inside)

    for j in range(4):
        at = 512 * j
        d1, d32, d64, d128 = segment_powers(j)
        to_seg = (jnp.ones((8, 512), F32), jnp.zeros((8, 512), F32))
        for bit, p in ((1, d32), (2, d64), (4, d128)):
            grown = complex_mul(to_seg, p)
            to_seg = tuple(jnp.where(seg // bit % 2 == 1, a, b) for a, b in zip(grown, to_seg))
        entering = tuple(
            jnp.broadcast_to(lanes_of(v[4 * j : 4 * j + 4, :]), (8, 512)) for v in incoming
        )
        h = complex_fma(to_seg, entering, (edge[0, :, at : at + 512], edge[1, :, at : at + 512]))
        half, base = j // 2, 512 * (j % 2)

        def double_step(i, h):
            rows = pl.ds(pl.multiple_of(i * 16, 16), 16)
            pr, pi = push[0, rows, at : at + 512], push[1, rows, at : at + 512]
            h = complex_fma(d1, h, (pr[0:8], pi[0:8]))
            g = complex_fma(d1, h, (pr[8:16], pi[8:16]))
            st[half, rows, base : base + 512] = jnp.concatenate([h[0], g[0]], axis=0).astype(BF16)
            st[half, rows, 1024 + base : 1536 + base] = jnp.concatenate(
                [h[1], g[1]], axis=0
            ).astype(BF16)
            return g

        lax.fori_loop(0, STEPS // 2, double_step, h, unroll=2)

    read = jnp.concatenate([dot(st[0], cblk[0]), dot(st[1], cblk[1])], axis=1)
    activated = jax.nn.gelu(read + skip_ref[...] * ordered.astype(F32)).astype(BF16)
    pre[k] = dot(unorder, activated).astype(BF16)
    pre_copy = remote(pre.at[k], pre.at[k], psend.at[2], precv.at[2], (c, other))
    pre_copy.start()

    loads[0].wait()
    lin = dot(pre[k], glu[pl.ds(pl.multiple_of(k * 512, 512), 512), :])
    pre_copy.wait()
    lin = lin + dot(pre[other], glu[pl.ds(pl.multiple_of(other * 512, 512), 512), :])
    full = jnp.concatenate([pre[0], pre[1]], axis=1).astype(F32)
    gated = (full * jax.nn.sigmoid(lin)).astype(BF16)
    loads[1].wait()
    loads[2].wait()
    res_copy.wait()
    squares = jnp.zeros((256, 1), F32)
    for n in range(4):
        cols = slice(512 * n, 512 * n + 512)
        start = jnp.concatenate([res[0, :, cols], res[1, :, cols]], axis=0).astype(F32)
        value = start + dot(gated, outw[:, cols])
        squares = squares + jnp.sum(value * value, axis=1, keepdims=True)
        mixed[:, cols] = value
    scale = lax.rsqrt(squares * (1.0 / 2048.0) + EPSILON)
    for n in range(4):
        cols = slice(512 * n, 512 * n + 512)
        normed[:, cols] = (mixed[:, cols] * scale * gain_ref[:, cols]).astype(BF16)
    for n in range(4):
        cols = slice(512 * n, 512 * n + 512)
        send[:, :, cols] = dot(hot[...], normed[:, cols]).reshape(64, 8, 512).astype(BF16)

    def dispatch(i, carry):
        q = i // PER_CHUNK
        remote(send.at[i], recv.at[i], ssem.at[q], rsem.at[q], (chip_at(i, 1), k)).start()
        return carry

    lax.fori_loop(1, 64, dispatch, 0)
    recv[0] = send[0]
    for n in (3, 4, 5):
        loads[n].wait()

    def arrived(buffer, sem, q, first):
        rows = pl.ds(q * PER_CHUNK + first, PER_CHUNK - first)
        return remote(buffer.at[rows], buffer.at[rows], sem.at[q], sem.at[q], (c, other))

    for q in range(CHUNKS):
        first = 1 if q == 0 else 0
        arrived(recv, rsem, q, first).wait_recv()
        rows_in = recv[PER_CHUNK * q : PER_CHUNK * q + PER_CHUNK].reshape(128, 2048)
        gate_part = dot(rows_in, wg[...])
        up_part = dot(rows_in, wu[...])
        hidden = (gate_part * jax.nn.sigmoid(gate_part) * up_part).astype(BF16)
        answer = dot(hidden, wd[...]).astype(BF16)
        ans[PER_CHUNK * q : PER_CHUNK * q + PER_CHUNK] = answer.reshape(PER_CHUNK, 8, 2048)

        def give_back(i, carry):
            remote(ans.at[i], ret.at[i], asem.at[q], bsem.at[q], (chip_at(i, -1), k)).start()
            return carry

        lax.fori_loop(PER_CHUNK * q + first, PER_CHUNK * q + PER_CHUNK, give_back, 0)
        if q == 0:
            ret[0] = ans[0]

    for q in range(CHUNKS):
        first = 1 if q == 0 else 0
        arrived(ret, bsem, q, first).wait_recv()
    returned = ret[...].reshape(512, 2048)
    theirs = comb[other]
    mine = comb[k]
    part_out[...] = (dot(theirs[:, 0:512], returned) + dot(theirs[:, 512:1024], returned)).astype(BF16)
    part_copy = remote(part_out, part_in, psend.at[3], precv.at[3], (c, other))
    part_copy.start()
    routed = dot(mine[:, 0:512], returned) + dot(mine[:, 512:1024], returned)
    routed = routed + mixed[pl.ds(pl.multiple_of(k * 128, 128), 128), :]
    part_copy.wait()
    o_ref[...] = (routed + part_in[...].astype(F32)).astype(BF16)

    def line_sent(target, carry):
        remote(line, ybuf.at[ln], ys.at[target], yr.at[ln], (target * 4 + x, k)).wait_send()
        return carry

    lax.fori_loop(ln + 1, 16, line_sent, 0)
    for q in range(CHUNKS):
        first = 1 if q == 0 else 0
        arrived(send, ssem, q, first).wait_send()
        arrived(ans, asem, q, first).wait_send()


def on_device(
    ssm_input, lam_real, lam_imag, state_in, read_out, channel_skip, glu_weight, out_weight,
    residual, norm_gain, expert_ids, route_weight, expert_gate, expert_up, expert_down,
):
    meta = jnp.concatenate(
        [
            expert_ids.T.astype(F32),
            route_weight.T,
            jnp.zeros((4, 128), F32),
            lam_real.reshape(16, 128),
            lam_imag.reshape(16, 128),
        ]
    )
    vmem = pl.BlockSpec(memory_space=pltpu.VMEM)
    hbm = pl.BlockSpec(memory_space=pl.ANY)
    dma = pltpu.SemaphoreType.DMA
    return pl.pallas_call(
        body,
        out_shape=jax.ShapeDtypeStruct((128, 2048), BF16),
        in_specs=[vmem] * 8 + [hbm] * 6,
        out_specs=vmem,
        scratch_shapes=[
            pltpu.VMEM((1024, 1024), BF16),
            pltpu.VMEM((1024, 2048), BF16),
            pltpu.VMEM((2, 128, 2048), BF16),
            pltpu.VMEM((2048, 512), BF16),
            pltpu.VMEM((2048, 512), BF16),
            pltpu.VMEM((512, 2048), BF16),
            pltpu.VMEM((8, 128), F32),
            pltpu.VMEM((2, 256, 2048), F32),
            pltpu.VMEM((2, 8, 2048), F32),
            pltpu.VMEM((2, 16, 128), F32),
            pltpu.VMEM((3, 2, 16, 128), F32),
            pltpu.VMEM((16, 2, 16, 128), F32),
            pltpu.VMEM((2, 16, 128), F32),
            pltpu.VMEM((2, 256, 2048), BF16),
            pltpu.VMEM((2, 2048, 256), BF16),
            pltpu.VMEM((512, 256), BF16),
            pltpu.VMEM((2, 128, 1024), BF16),
            pltpu.VMEM((2, 256, 512), BF16),
            pltpu.VMEM((256, 2048), F32),
            pltpu.VMEM((256, 2048), BF16),
            pltpu.VMEM((64, 8, 2048), BF16),
            pltpu.VMEM((64, 8, 2048), BF16),
            pltpu.VMEM((64, 8, 2048), BF16),
            pltpu.VMEM((64, 8, 2048), BF16),
            pltpu.VMEM((128, 2048), BF16),
            pltpu.VMEM((128, 2048), BF16),
            dma((6,)), dma((3,)), dma((3,)), dma((16,)), dma((16,)), dma((4,)), dma((4,)),
            dma((4,)), dma((4,)), dma((4,)), dma((4,)),
        ],
        compiler_params=pltpu.CompilerParams(
            collective_id=0, has_side_effects=True, vmem_limit_bytes=60 * 1024 * 1024
        ),
    )(
        ssm_input, lam_real, lam_imag, state_in.reshape(2, 512, 64), read_out,
        channel_skip.reshape(1, 512), norm_gain.reshape(1, 2048), meta,
        glu_weight, out_weight, residual, expert_gate, expert_up, expert_down,
    )


def solution(mesh):
    both = P(("sp", "tp"), None)
    each = P(("sp", "tp"), None, None)
    in_specs = (
        P("sp", "tp"), P("tp", None), P("tp", None), P(None, "tp", None, None), P("tp", None, None),
        P("tp"), P(), P(), both, P(), both, both, each, each, each,
    )
    return jax.shard_map(on_device, mesh=mesh, in_specs=in_specs, out_specs=both, check_vma=False)
```

time: 634 us -> 106 us (0.17); the launches traced: 621 us -> 106 us
  local copies, waits for them, and re-layouts: 398 us -> 8.85 us
  Pallas kernels: 0 us -> 96.2 us
  other arithmetic: 74.7 us -> 0.68 us
  blocking collectives: 70.4 us -> 0 us
  waiting for transfers between devices: 30.1 us -> 0 us
  matrix products: 28.8 us -> 0 us
  starting transfers between devices: 17.9 us -> 0 us
    slice x54 -> x0, local copies, waits for them, and re-layouts: 286 us -> none  [the longest x53 283 us: block_states(): lax.associative_scan(combine_steps, (scale_re, scale_im, flat_re, flat_im...]
    pallas_call x0 -> x1, Pallas kernels: none -> 96.2 us  [on_device(): pl.pallas_call(body, out_shape=jax.ShapeDtypeStruct((128, 2048), BF16), i...]
    pad x28 -> x0, local copies, waits for them, and re-layouts: 49.8 us -> none  [block_states(): lax.associative_scan(combine_steps, (scale_re, scale_im, flat_re, flat_im...]
    all_to_all x1 -> x0, blocking collectives: 38.3 us -> none  [on_device(): lax.all_to_all(outgoing, SP_TP, split_axis=0, concat_axis=0, tiled=True)]
    add x40 -> x0, other arithmetic: 35.8 us -> none  [the longest x17 19.2 us: block_states(): lax.associative_scan(combine_steps, (scale_re, scale_im, flat_re, flat_im...]
    all_gather x3 -> x0, blocking collectives: 32.2 us -> none  [collected_together(): both, at, found = (lax.all_gather(jnp.concatenate(lines), axis), 0, {})]
    all_to_all x2 -> x0, waiting for transfers between devices: 30.1 us -> none  [the longest x1 30.1 us: on_device(): lax.all_to_all(answered, SP_TP, split_axis=0, concat_axis=0, tiled=True)]
    dot_general x6 -> x0, matrix products: 28.8 us -> none  [the longest x2 12 us: readout(): jnp.einsum('tgq,gqm->tgm', stacked, read_out, precision=lax.Precision.HIG...]
  transfers between devices with their start and end apart: 2 -> 0, of which waited for: 1 -> 0; matrix products, arithmetic and copies ran while one was open for 1% -> 0% of each run, Pallas kernels for 0% -> 0%
where the time goes in v1:
time: 106 us
  Pallas kernels  96.2 us (91%)
  local copies, waits for them, and re-layouts  8.85 us (8%)
    pallas_call x1, Pallas kernels, on_device(): pl.pallas_call(body, out_shape=jax.ShapeDtypeStruct((128, 2048), BF16), i...  96.2 us
    unnamed x2, local copies, waits for them, and re-layouts  4.79 us
    concatenate x1, local copies, waits for them, and re-layouts, on_device(): jnp.concatenate([expert_ids.T.astype(F32), route_weight.T, jnp.zeros((4,...  2.48 us

profile of v1, /device:TPU:1, one launch (start us, length us, event | category | flops | bytes accessed | tf_op | source)
XLA Modules:
  0.0 105.7 jit_solution(4481190572379966396)
XLA Ops:
  0.0 0.7 convert_bitcast_fusion
  0.7 0.8 reshape.18
  1.5 0.8 reshape.19
  2.3 2.5 %concatenate.3.meta_ref = f32[40,128]{1,0:T(8,128)} concatenate(f32[2,128]{1,0:T(2,128)S(1)} %convert_bitcast_fusion, f32[2,128]{1,0:T(2,128)} %bitcast.9, f32[4,128]{1,0:T(4,128)S(1)} %broadcast_in_dim.3, f32[16,128]{1,0:T(8,128)S(1)} %reshape.18, f32[16,128]{1,0:T(8,128)S(1)} %reshape.19), dimensions={0} | concatenate | bytes 40960 | tf_op jit(solution)/shard_map/concatenate | solution.py:352
  4.7 2.9 %copy.16.ro_ref = f32[32,128,16]{2,1,0:T(8,128)} copy(f32[32,128,16]{1,2,0:T(8,128)} %param.19) | data formatting | bytes 524288 | tf_op args[4]
  7.6 96.2 %shard_map.145 = bf16[128,2048]{1,0:T(8,128)(2,1)} custom-call(bf16[256,512]{1,0:T(8,128)(2,1)} %u_ref.1, f32[32,64]{1,0:T(8,128)} %lr_ref.1, f32[32,64]{1,0:T(8,128)} %li_ref.1, f32[2,512,64]{2,1,0:T(8,128)} %bitcast.6, f32[32,128,16]{2,1,0:T(8,128)} %copy.16.ro_ref, f32[1,512]{1,0:T(1,128)} %bitcast.8, f32[1,2048]{1,0:T(1,128)} %bitcast.7, ...), custom_call_target="tpu_custom_call" | custom-call | tf_op jit(solution)/shard_map/pallas_call | solution.py:364
  103.8 1.9 %copy.18 = bf16[128,2048]{1,0:T(8,128)(2,1)} copy(bf16[128,2048]{1,0:T(8,128)(2,1)} %shard_map.145) | data formatting | bytes 1048576
  (1 shorter events, 0.0 us)

commit v2 on v1

--- a/solution.py
+++ b/solution.py
@@ -21,6 +21,10 @@
     return jnp.dot(a, b, preferred_element_type=F32)
 
 
+def dot_t(a, b):
+    return lax.dot_general(a, b, (((1,), (1,)), ((), ())), preferred_element_type=F32)
+
+
 def iota(shape, dim):
     return lax.broadcasted_iota(jnp.int32, shape, dim)
 
@@ -46,10 +50,10 @@
 
 
 def body(
-    u_ref, lr_ref, li_ref, in_ref, ro_ref, skip_ref, gain_ref, meta_ref,
+    u_ref, lr_ref, li_ref, in_ref, ro_ref, skip_ref, gain_ref, ids_ref, rw_ref,
     glu_hbm, outw_hbm, res_hbm, wg_hbm, wu_hbm, wd_hbm,
     o_ref,
-    glu, outw, res, wg, wu, wd, meta2,
+    glu, outw, res, wg, wu, wd, ids2, rw2,
     push, edge, fin, xbuf, ybuf, line, st, cblk, hot, comb,
     pre, mixed, normed, send, recv, ans, ret, part_out, part_in,
     hsem, xs, xr, ys, yr, psend, precv, ssem, rsem, asem, bsem,
@@ -112,7 +116,10 @@
                 ordered[:, 256 * half : 256 * half + 256], block
             )
 
-    dense_r, dense_i = meta_ref[8:24, :], meta_ref[24:40, :]
+    def dense(ref):
+        return jnp.concatenate([ref[pl.ds(n, 16, stride=2), :] for n in range(2)], axis=1)
+
+    dense_r, dense_i = dense(lr_ref), dense(li_ref)
     p1 = power(dense_r, dense_i, 1.0)
     p32 = power(dense_r, dense_i, 32.0)
     p64 = power(dense_r, dense_i, 64.0)
@@ -161,18 +168,18 @@
     ]
     for copy in along:
         copy.start()
-    meta_copy = remote(meta_ref.at[0:8], meta2, psend.at[0], precv.at[0], (c, other))
-    meta_copy.start()
+    ids_copy = remote(ids_ref, ids2, psend.at[0], precv.at[0], (c, other))
+    ids_copy.start()
+    rw_copy = remote(rw_ref, rw2, psend.at[4], precv.at[4], (c, other))
+    rw_copy.start()
     res_copy = remote(res_hbm, res.at[k], psend.at[1], precv.at[1], (c, other))
     res_copy.start()
 
-    narrow = (iota((16, 256), 1) % 16 == iota((16, 256), 0)).astype(F32).astype(BF16)
-    own_read = iota((1024, 256), 0) // 64 == iota((1024, 256), 1) // 16
     for half in range(2):
         for part in range(2):
-            piece = ro_ref[16 * half : 16 * half + 16, 64 * part : 64 * part + 64, :]
-            piece = dot(piece.reshape(1024, 16).astype(BF16), narrow)
-            cblk[half, 1024 * part : 1024 * part + 1024, :] = jnp.where(own_read, piece, 0.0).astype(BF16)
+            piece = ro_ref[16 * half : 16 * half + 16, :, 64 * part : 64 * part + 64]
+            piece = dot(piece.reshape(256, 64).astype(BF16), spread)
+            cblk[half, :, 1024 * part : 1024 * part + 1024] = jnp.where(own_block, piece, 0.0).astype(BF16)
 
     for copy in along:
         copy.wait()
@@ -200,23 +207,24 @@
 
     lax.fori_loop(ln + 1, 16, to_line, 0)
 
-    meta_copy.wait()
+    ids_copy.wait()
+    rw_copy.wait()
     slot = iota((64, 128), 0)
     chip = (
         ((z + slot // 16) % 4) * 16 + ((y + (slot // 4) % 4) % 4) * 4 + (x + slot % 4) % 4
     )
-    expert = (chip * 2 + k).astype(F32)
+    expert = chip * 2 + k
     before = (iota((128, 128), 0) < iota((128, 128), 1)).astype(F32).astype(BF16)
     sub = iota((64, 8, 128), 1)
-    own_meta, other_meta = meta_ref[0:8, :], meta2[...]
     for b in range(2):
-        m = jnp.where(k == b, own_meta, other_meta)
-        first = m[0:1, :] == expert
-        second = m[1:2, :] == expert
+        ids = jnp.where(k == b, ids_ref[...], ids2[...])
+        weights = jnp.where(k == b, rw_ref[...], rw2[...])
+        first = ids[0:1, :] == expert
+        second = ids[1:2, :] == expert
         named = jnp.logical_or(first, second)
         rank = dot(named.astype(F32).astype(BF16), before)
         rank = jnp.where(named, rank + 4.0 * b, -1.0)
-        weight = jnp.where(first, m[2:3, :], m[3:4, :])
+        weight = jnp.where(first, weights[0:1, :], weights[1:2, :])
         hit = rank[:, None, :] == sub.astype(F32)
         hot[:, 128 * b : 128 * b + 128] = hit.astype(F32).reshape(512, 128).astype(BF16)
         scaled = jnp.where(hit, weight[:, None, :], 0.0).reshape(512, 128)
@@ -258,7 +266,7 @@
 
         lax.fori_loop(0, STEPS // 2, double_step, h, unroll=2)
 
-    read = jnp.concatenate([dot(st[0], cblk[0]), dot(st[1], cblk[1])], axis=1)
+    read = jnp.concatenate([dot_t(st[0], cblk[0]), dot_t(st[1], cblk[1])], axis=1)
     activated = jax.nn.gelu(read + skip_ref[...] * ordered.astype(F32)).astype(BF16)
     pre[k] = dot(unorder, activated).astype(BF16)
     pre_copy = remote(pre.at[k], pre.at[k], psend.at[2], precv.at[2], (c, other))
@@ -349,22 +357,13 @@
     ssm_input, lam_real, lam_imag, state_in, read_out, channel_skip, glu_weight, out_weight,
     residual, norm_gain, expert_ids, route_weight, expert_gate, expert_up, expert_down,
 ):
-    meta = jnp.concatenate(
-        [
-            expert_ids.T.astype(F32),
-            route_weight.T,
-            jnp.zeros((4, 128), F32),
-            lam_real.reshape(16, 128),
-            lam_imag.reshape(16, 128),
-        ]
-    )
     vmem = pl.BlockSpec(memory_space=pltpu.VMEM)
     hbm = pl.BlockSpec(memory_space=pl.ANY)
     dma = pltpu.SemaphoreType.DMA
     return pl.pallas_call(
         body,
         out_shape=jax.ShapeDtypeStruct((128, 2048), BF16),
-        in_specs=[vmem] * 8 + [hbm] * 6,
+        in_specs=[vmem] * 9 + [hbm] * 6,
         out_specs=vmem,
         scratch_shapes=[
             pltpu.VMEM((1024, 1024), BF16),
@@ -373,7 +372,8 @@
             pltpu.VMEM((2048, 512), BF16),
             pltpu.VMEM((2048, 512), BF16),
             pltpu.VMEM((512, 2048), BF16),
-            pltpu.VMEM((8, 128), F32),
+            pltpu.VMEM((2, 128), jnp.int32),
+            pltpu.VMEM((2, 128), F32),
             pltpu.VMEM((2, 256, 2048), F32),
             pltpu.VMEM((2, 8, 2048), F32),
             pltpu.VMEM((2, 16, 128), F32),
@@ -381,7 +381,7 @@
             pltpu.VMEM((16, 2, 16, 128), F32),
             pltpu.VMEM((2, 16, 128), F32),
             pltpu.VMEM((2, 256, 2048), BF16),
-            pltpu.VMEM((2, 2048, 256), BF16),
+            pltpu.VMEM((2, 256, 2048), BF16),
             pltpu.VMEM((512, 256), BF16),
             pltpu.VMEM((2, 128, 1024), BF16),
             pltpu.VMEM((2, 256, 512), BF16),
@@ -393,15 +393,16 @@
             pltpu.VMEM((64, 8, 2048), BF16),
             pltpu.VMEM((128, 2048), BF16),
             pltpu.VMEM((128, 2048), BF16),
-            dma((6,)), dma((3,)), dma((3,)), dma((16,)), dma((16,)), dma((4,)), dma((4,)),
+            dma((6,)), dma((3,)), dma((3,)), dma((16,)), dma((16,)), dma((5,)), dma((5,)),
             dma((4,)), dma((4,)), dma((4,)), dma((4,)),
         ],
         compiler_params=pltpu.CompilerParams(
             collective_id=0, has_side_effects=True, vmem_limit_bytes=60 * 1024 * 1024
         ),
     )(
-        ssm_input, lam_real, lam_imag, state_in.reshape(2, 512, 64), read_out,
-        channel_skip.reshape(1, 512), norm_gain.reshape(1, 2048), meta,
+        ssm_input, lam_real, lam_imag, state_in.reshape(2, 512, 64),
+        read_out.transpose(0, 2, 1), channel_skip.reshape(1, 512), norm_gain.reshape(1, 2048),
+        expert_ids.T, route_weight.T,
         glu_weight, out_weight, residual, expert_gate, expert_up, expert_down,
     )
 

time: 106 us -> 97.3 us (0.918)
  local copies, waits for them, and re-layouts: 8.85 us -> 1.88 us
    unnamed x2 -> x1, local copies, waits for them, and re-layouts: 4.79 us -> 1.88 us
    concatenate x1 -> x0, local copies, waits for them, and re-layouts: 2.48 us -> none  [on_device(): jnp.concatenate([expert_ids.T.astype(F32), route_weight.T, jnp.zeros((4,...]
    reshape x2 -> x0, local copies, waits for them, and re-layouts: 1.57 us -> none  [the longest x1 0.79 us: on_device(): lam_imag.reshape(16, 128)]
where the time goes in v2:
time: 97.3 us; the launch traced here: 97.1 us
  Pallas kernels  95.2 us (98%)
  local copies, waits for them, and re-layouts  1.88 us (2%)
    pallas_call x1, Pallas kernels, on_device(): pl.pallas_call(body, out_shape=jax.ShapeDtypeStruct((128, 2048), BF16), i...  95.2 us

profile of v2, /device:TPU:1, one launch (start us, length us, event | category | flops | bytes accessed | tf_op | source)
XLA Modules:
  0.0 97.1 jit_solution(1450454400981711739)
XLA Ops:
  0.0 95.2 %shard_map.145 = bf16[128,2048]{1,0:T(8,128)(2,1)} custom-call(bf16[256,512]{1,0:T(8,128)(2,1)} %u_ref.1, f32[32,64]{1,0:T(8,128)} %lr_ref.1, f32[32,64]{1,0:T(8,128)} %li_ref.1, f32[2,512,64]{2,1,0:T(8,128)} %bitcast.6, f32[32,16,128]{2,1,0:T(8,128)} %bitcast.7, f32[1,512]{1,0:T(1,128)} %bitcast.9, f32[1,2048]{1,0:T(1,128)} %bitcast.8, s32[2,128]{1,0:T(2,128)} %bitcast.10, ...), custom_call_target="tpu_custom_call" | custom-call | tf_op jit(solution)/shard_map/pallas_call | solution.py:363
  95.2 1.9 %copy.17 = bf16[128,2048]{1,0:T(8,128)(2,1)} copy(bf16[128,2048]{1,0:T(8,128)(2,1)} %shard_map.145) | data formatting | bytes 1048576

commit v3 on v2

--- a/solution.py
+++ b/solution.py
@@ -17,6 +17,32 @@
 PER_CHUNK = 16
 
 
+def steps_of(shift):
+    both = []
+    for d in shift:
+        both += [float(d == 1) + float(d == 2), float(d == 3) + float(d == 2)]
+    return both
+
+
+def balanced_order():
+    left = [(n // 16, n // 4 % 4, n % 4) for n in range(1, 64)]
+    total, order = [0.0] * 6, [(0, 0, 0)]
+    while left:
+
+        def cost(shift):
+            now = [a + b for a, b in zip(total, steps_of(shift))]
+            return (max(now) - min(now), -sum(steps_of(shift)))
+
+        best = min(left, key=cost)
+        left.remove(best)
+        order.append(best)
+        total = [a + b for a, b in zip(total, steps_of(best))]
+    return order
+
+
+ORDER = balanced_order()
+
+
 def dot(a, b):
     return jnp.dot(a, b, preferred_element_type=F32)
 
@@ -55,7 +81,7 @@
     o_ref,
     glu, outw, res, wg, wu, wd, ids2, rw2,
     push, edge, fin, xbuf, ybuf, line, st, cblk, hot, comb,
-    pre, mixed, normed, send, recv, ans, ret, part_out, part_in,
+    pre, mixed, normed, send, recv, ans, ret, part_out, part_in, part_sum, own_sum,
     hsem, xs, xr, ys, yr, psend, precv, ssem, rsem, asem, bsem,
 ):
     c = lax.axis_index("sp")
@@ -64,11 +90,9 @@
     z, y, x = c // 16, (c // 4) % 4, c % 4
     ln = c // 4
 
-    def chip_at(i, sign):
-        dz, dy, dx = i // 16, (i // 4) % 4, i % 4
-        return (
-            ((z + sign * dz + 4) % 4) * 16 + ((y + sign * dy + 4) % 4) * 4 + (x + sign * dx + 4) % 4
-        )
+    def chip_at(shift, sign):
+        dz, dy, dx = (sign * d % 4 for d in shift)
+        return ((z + dz) % 4) * 16 + ((y + dy) % 4) * 4 + (x + dx) % 4
 
     loads = [
         pltpu.make_async_copy(glu_hbm, glu, hsem.at[0]),
@@ -84,11 +108,10 @@
     barrier = pltpu.get_barrier_semaphore()
     pl.semaphore_signal(barrier, inc=1, device_id=(c, other), device_id_type=MESH)
 
-    def greet(i, carry):
-        pl.semaphore_signal(barrier, inc=1, device_id=(chip_at(i, 1), k), device_id_type=MESH)
-        return carry
-
-    lax.fori_loop(1, 64, greet, 0)
+    for d in (1, 2, 3):
+        pl.semaphore_signal(barrier, inc=1, device_id=(c - x + (x + d) % 4, k), device_id_type=MESH)
+    for d in range(1, 16):
+        pl.semaphore_signal(barrier, inc=1, device_id=((c + 4 * d) % 64, k), device_id_type=MESH)
 
     lam_r, lam_i = lr_ref[...], li_ref[...]
     decay_re, decay_im = power(lam_r, lam_i, 1.0)
@@ -155,7 +178,7 @@
             for n in range(4):
                 fin[part, 4 * j + n : 4 * j + n + 1, :] = h[part][7:8, 128 * n : 128 * n + 128]
 
-    pl.semaphore_wait(barrier, 64)
+    pl.semaphore_wait(barrier, 19)
 
     def remote(src, dst, s, r, device):
         return pltpu.make_async_remote_copy(
@@ -210,9 +233,10 @@
     ids_copy.wait()
     rw_copy.wait()
     slot = iota((64, 128), 0)
-    chip = (
-        ((z + slot // 16) % 4) * 16 + ((y + (slot // 4) % 4) % 4) * 4 + (x + slot % 4) % 4
-    )
+    code = jnp.zeros((64, 128), jnp.int32)
+    for n, (dz, dy, dx) in enumerate(ORDER):
+        code = jnp.where(slot == n, dz * 16 + dy * 4 + dx, code)
+    chip = ((z + code // 16) % 4) * 16 + ((y + code // 4 % 4) % 4) * 4 + (x + code % 4) % 4
     expert = chip * 2 + k
     before = (iota((128, 128), 0) < iota((128, 128), 1)).astype(F32).astype(BF16)
     sub = iota((64, 8, 128), 1)
@@ -296,51 +320,52 @@
         cols = slice(512 * n, 512 * n + 512)
         send[:, :, cols] = dot(hot[...], normed[:, cols]).reshape(64, 8, 512).astype(BF16)
 
-    def dispatch(i, carry):
-        q = i // PER_CHUNK
-        remote(send.at[i], recv.at[i], ssem.at[q], rsem.at[q], (chip_at(i, 1), k)).start()
-        return carry
-
-    lax.fori_loop(1, 64, dispatch, 0)
+    for n in range(1, 64):
+        q = n // PER_CHUNK
+        remote(send.at[n], recv.at[n], ssem.at[q], rsem.at[q], (chip_at(ORDER[n], 1), k)).start()
     recv[0] = send[0]
     for n in (3, 4, 5):
         loads[n].wait()
 
-    def arrived(buffer, sem, q, first):
+    def arrived(buffer, sem, q):
+        first = 1 if q == 0 else 0
         rows = pl.ds(q * PER_CHUNK + first, PER_CHUNK - first)
         return remote(buffer.at[rows], buffer.at[rows], sem.at[q], sem.at[q], (c, other))
 
     for q in range(CHUNKS):
-        first = 1 if q == 0 else 0
-        arrived(recv, rsem, q, first).wait_recv()
-        rows_in = recv[PER_CHUNK * q : PER_CHUNK * q + PER_CHUNK].reshape(128, 2048)
+        arrived(recv, rsem, q).wait_recv()
+        slots = slice(PER_CHUNK * q, PER_CHUNK * q + PER_CHUNK)
+        rows_in = recv[slots].reshape(8 * PER_CHUNK, 2048)
         gate_part = dot(rows_in, wg[...])
         up_part = dot(rows_in, wu[...])
         hidden = (gate_part * jax.nn.sigmoid(gate_part) * up_part).astype(BF16)
-        answer = dot(hidden, wd[...]).astype(BF16)
-        ans[PER_CHUNK * q : PER_CHUNK * q + PER_CHUNK] = answer.reshape(PER_CHUNK, 8, 2048)
-
-        def give_back(i, carry):
-            remote(ans.at[i], ret.at[i], asem.at[q], bsem.at[q], (chip_at(i, -1), k)).start()
-            return carry
-
-        lax.fori_loop(PER_CHUNK * q + first, PER_CHUNK * q + PER_CHUNK, give_back, 0)
+        ans[slots] = dot(hidden, wd[...]).astype(BF16).reshape(PER_CHUNK, 8, 2048)
+        for n in range(max(1, PER_CHUNK * q), PER_CHUNK * q + PER_CHUNK):
+            remote(ans.at[n], ret.at[n], asem.at[q], bsem.at[q], (chip_at(ORDER[n], -1), k)).start()
         if q == 0:
             ret[0] = ans[0]
 
-    for q in range(CHUNKS):
-        first = 1 if q == 0 else 0
-        arrived(ret, bsem, q, first).wait_recv()
-    returned = ret[...].reshape(512, 2048)
-    theirs = comb[other]
-    mine = comb[k]
-    part_out[...] = (dot(theirs[:, 0:512], returned) + dot(theirs[:, 512:1024], returned)).astype(BF16)
-    part_copy = remote(part_out, part_in, psend.at[3], precv.at[3], (c, other))
-    part_copy.start()
-    routed = dot(mine[:, 0:512], returned) + dot(mine[:, 512:1024], returned)
-    routed = routed + mixed[pl.ds(pl.multiple_of(k * 128, 128), 128), :]
+    for half in range(2):
+        for q in range(half * CHUNKS // 2, (half + 1) * CHUNKS // 2):
+            arrived(ret, bsem, q).wait_recv()
+        returned = ret[32 * half : 32 * half + 32].reshape(256, 2048)
+        high = slice(256 * half, 256 * half + 256)
+        low = slice(512 + 256 * half, 768 + 256 * half)
+        theirs, mine = comb[other], comb[k]
+        routed = dot(theirs[:, high], returned) + dot(theirs[:, low], returned)
+        if half == 0:
+            part_sum[...] = routed
+            own_rows = pl.ds(pl.multiple_of(k * 128, 128), 128)
+            own_sum[...] = (
+                mixed[own_rows, :] + dot(mine[:, high], returned) + dot(mine[:, low], returned)
+            )
+        else:
+            part_out[...] = (part_sum[...] + routed).astype(BF16)
+            part_copy = remote(part_out, part_in, psend.at[3], precv.at[3], (c, other))
+            part_copy.start()
+            own_sum[...] = own_sum[...] + dot(mine[:, high], returned) + dot(mine[:, low], returned)
     part_copy.wait()
-    o_ref[...] = (routed + part_in[...].astype(F32)).astype(BF16)
+    o_ref[...] = (own_sum[...] + part_in[...].astype(F32)).astype(BF16)
 
     def line_sent(target, carry):
         remote(line, ybuf.at[ln], ys.at[target], yr.at[ln], (target * 4 + x, k)).wait_send()
@@ -348,9 +373,8 @@
 
     lax.fori_loop(ln + 1, 16, line_sent, 0)
     for q in range(CHUNKS):
-        first = 1 if q == 0 else 0
-        arrived(send, ssem, q, first).wait_send()
-        arrived(ans, asem, q, first).wait_send()
+        arrived(send, ssem, q).wait_send()
+        arrived(ans, asem, q).wait_send()
 
 
 def on_device(
@@ -393,6 +417,8 @@
             pltpu.VMEM((64, 8, 2048), BF16),
             pltpu.VMEM((128, 2048), BF16),
             pltpu.VMEM((128, 2048), BF16),
+            pltpu.VMEM((128, 2048), F32),
+            pltpu.VMEM((128, 2048), F32),
             dma((6,)), dma((3,)), dma((3,)), dma((16,)), dma((16,)), dma((5,)), dma((5,)),
             dma((4,)), dma((4,)), dma((4,)), dma((4,)),
         ],

time: 97.3 us -> 89 us (0.915)
  the two profiles are of different devices: /device:TPU:1 before, /device:TPU:11 now
where the time goes in v3:
time: 89 us; the launch traced here: 88.8 us
  Pallas kernels  86.9 us (98%)
  local copies, waits for them, and re-layouts  1.88 us (2%)
    pallas_call x1, Pallas kernels, on_device(): pl.pallas_call(body, out_shape=jax.ShapeDtypeStruct((128, 2048), BF16), i...  86.9 us
    unnamed x1, local copies, waits for them, and re-layouts  1.88 us

profile of v3, /device:TPU:11, one launch (start us, length us, event | category | flops | bytes accessed | tf_op | source)
XLA Modules:
  0.0 88.8 jit_solution(6105484012858051681)
XLA Ops:
  0.0 86.9 %shard_map.145 = bf16[128,2048]{1,0:T(8,128)(2,1)} custom-call(bf16[256,512]{1,0:T(8,128)(2,1)} %u_ref.1, f32[32,64]{1,0:T(8,128)} %lr_ref.1, f32[32,64]{1,0:T(8,128)} %li_ref.1, f32[2,512,64]{2,1,0:T(8,128)} %bitcast.6, f32[32,16,128]{2,1,0:T(8,128)} %bitcast.7, f32[1,512]{1,0:T(1,128)} %bitcast.9, f32[1,2048]{1,0:T(1,128)} %bitcast.8, s32[2,128]{1,0:T(2,128)} %bitcast.10, ...), custom_call_target="tpu_custom_call" | custom-call | tf_op jit(solution)/shard_map/pallas_call | solution.py:387
  86.9 1.9 %copy.17 = bf16[128,2048]{1,0:T(8,128)(2,1)} copy(bf16[128,2048]{1,0:T(8,128)(2,1)} %shard_map.145) | data formatting | bytes 1048576

commit v4 on v3

--- a/solution.py
+++ b/solution.py
@@ -15,6 +15,8 @@
 STEPS = 32
 CHUNKS = 4
 PER_CHUNK = 16
+EARLY = 1
+EARLY_SLOTS = EARLY * PER_CHUNK
 
 
 def steps_of(shift):
@@ -81,8 +83,8 @@
     o_ref,
     glu, outw, res, wg, wu, wd, ids2, rw2,
     push, edge, fin, xbuf, ybuf, line, st, cblk, hot, comb,
-    pre, mixed, normed, send, recv, ans, ret, part_out, part_in, part_sum, own_sum,
-    hsem, xs, xr, ys, yr, psend, precv, ssem, rsem, asem, bsem,
+    pre, mixed, normed, send, recv, ans, ret, part_out, part_in, part_sum, own_sum, gsend, grecv,
+    hsem, xs, xr, ys, yr, psend, precv, ssem, rsem, asem, bsem, gsem, grsem,
 ):
     c = lax.axis_index("sp")
     k = lax.axis_index("tp")
@@ -257,6 +259,20 @@
         comb[b, :, 0:512] = high
         comb[b, :, 512:1024] = (scaled - high.astype(F32)).astype(BF16)
 
+    loads[2].wait()
+    res_copy.wait()
+    for n in range(4):
+        cols = slice(512 * n, 512 * n + 512)
+        rows = jnp.concatenate([res[0, :, cols], res[1, :, cols]], axis=0)
+        send[0:EARLY_SLOTS, :, cols] = (
+            dot(hot[0 : 8 * EARLY_SLOTS], rows).reshape(EARLY_SLOTS, 8, 512).astype(BF16)
+        )
+
+    def send_rows(first, last):
+        for n in range(max(1, first), last):
+            q = n // PER_CHUNK
+            remote(send.at[n], recv.at[n], ssem.at[q], rsem.at[q], (chip_at(ORDER[n], 1), k)).start()
+
     def from_line(n, acc):
         remote(line, ybuf.at[n], ys.at[0], yr.at[n], (c, other)).wait_recv()
         return complex_fma(q4, acc, (ybuf[n, 0], ybuf[n, 1]))
@@ -296,15 +312,23 @@
     pre_copy = remote(pre.at[k], pre.at[k], psend.at[2], precv.at[2], (c, other))
     pre_copy.start()
 
+    send_rows(1, 16)
+
     loads[0].wait()
     lin = dot(pre[k], glu[pl.ds(pl.multiple_of(k * 512, 512), 512), :])
     pre_copy.wait()
     lin = lin + dot(pre[other], glu[pl.ds(pl.multiple_of(other * 512, 512), 512), :])
     full = jnp.concatenate([pre[0], pre[1]], axis=1).astype(F32)
     gated = (full * jax.nn.sigmoid(lin)).astype(BF16)
+    for n in range(2):
+        cols = slice(512 * n, 512 * n + 512)
+        gsend[:, :, cols] = (
+            dot(hot[0 : 8 * EARLY_SLOTS], gated[:, cols]).reshape(EARLY_SLOTS, 8, 512).astype(BF16)
+        )
+    for n in range(1, EARLY_SLOTS):
+        q = n // PER_CHUNK
+        remote(gsend.at[n], grecv.at[n], gsem.at[q], grsem.at[q], (chip_at(ORDER[n], 1), k)).start()
     loads[1].wait()
-    loads[2].wait()
-    res_copy.wait()
     squares = jnp.zeros((256, 1), F32)
     for n in range(4):
         cols = slice(512 * n, 512 * n + 512)
@@ -318,12 +342,15 @@
         normed[:, cols] = (mixed[:, cols] * scale * gain_ref[:, cols]).astype(BF16)
     for n in range(4):
         cols = slice(512 * n, 512 * n + 512)
-        send[:, :, cols] = dot(hot[...], normed[:, cols]).reshape(64, 8, 512).astype(BF16)
-
-    for n in range(1, 64):
-        q = n // PER_CHUNK
-        remote(send.at[n], recv.at[n], ssem.at[q], rsem.at[q], (chip_at(ORDER[n], 1), k)).start()
+        send[EARLY_SLOTS:64, :, cols] = (
+            dot(hot[8 * EARLY_SLOTS : 512], normed[:, cols])
+            .reshape(64 - EARLY_SLOTS, 8, 512)
+            .astype(BF16)
+        )
+
+    send_rows(EARLY_SLOTS, 64)
     recv[0] = send[0]
+    grecv[0] = gsend[0]
     for n in (3, 4, 5):
         loads[n].wait()
 
@@ -334,8 +361,14 @@
 
     for q in range(CHUNKS):
         arrived(recv, rsem, q).wait_recv()
+        if q < EARLY:
+            arrived(grecv, grsem, q).wait_recv()
         slots = slice(PER_CHUNK * q, PER_CHUNK * q + PER_CHUNK)
         rows_in = recv[slots].reshape(8 * PER_CHUNK, 2048)
+        if q < EARLY:
+            early = dot(grecv[slots].reshape(8 * PER_CHUNK, 1024), outw[...]) + rows_in.astype(F32)
+            mean = jnp.sum(early * early, axis=1, keepdims=True) * (1.0 / 2048.0)
+            rows_in = (early * lax.rsqrt(mean + EPSILON) * gain_ref[...]).astype(BF16)
         gate_part = dot(rows_in, wg[...])
         up_part = dot(rows_in, wu[...])
         hidden = (gate_part * jax.nn.sigmoid(gate_part) * up_part).astype(BF16)
@@ -374,6 +407,8 @@
     lax.fori_loop(ln + 1, 16, line_sent, 0)
     for q in range(CHUNKS):
         arrived(send, ssem, q).wait_send()
+        if q < EARLY:
+            arrived(gsend, gsem, q).wait_send()
         arrived(ans, asem, q).wait_send()
 
 
@@ -419,8 +454,10 @@
             pltpu.VMEM((128, 2048), BF16),
             pltpu.VMEM((128, 2048), F32),
             pltpu.VMEM((128, 2048), F32),
+            pltpu.VMEM((EARLY_SLOTS, 8, 1024), BF16),
+            pltpu.VMEM((EARLY_SLOTS, 8, 1024), BF16),
             dma((6,)), dma((3,)), dma((3,)), dma((16,)), dma((16,)), dma((5,)), dma((5,)),
-            dma((4,)), dma((4,)), dma((4,)), dma((4,)),
+            dma((4,)), dma((4,)), dma((4,)), dma((4,)), dma((EARLY,)), dma((EARLY,)),
         ],
         compiler_params=pltpu.CompilerParams(
             collective_id=0, has_side_effects=True, vmem_limit_bytes=60 * 1024 * 1024

time: 89 us -> 79.3 us (0.89)
  the two profiles are of different devices: /device:TPU:11 before, /device:TPU:1 now
where the time goes in v4:
time: 79.3 us; the launch traced here: 79.1 us
  Pallas kernels  77.2 us (97%)
  local copies, waits for them, and re-layouts  1.88 us (2%)
    pallas_call x1, Pallas kernels, on_device(): pl.pallas_call(body, out_shape=jax.ShapeDtypeStruct((128, 2048), BF16), i...  77.2 us
    unnamed x1, local copies, waits for them, and re-layouts  1.88 us

profile of v4, /device:TPU:1, one launch (start us, length us, event | category | flops | bytes accessed | tf_op | source)
XLA Modules:
  0.0 79.1 jit_solution(13535492807529817688)
XLA Ops:
  0.0 77.2 %shard_map.145 = bf16[128,2048]{1,0:T(8,128)(2,1)} custom-call(bf16[256,512]{1,0:T(8,128)(2,1)} %u_ref.1, f32[32,64]{1,0:T(8,128)} %lr_ref.1, f32[32,64]{1,0:T(8,128)} %li_ref.1, f32[2,512,64]{2,1,0:T(8,128)} %bitcast.6, f32[32,16,128]{2,1,0:T(8,128)} %bitcast.7, f32[1,512]{1,0:T(1,128)} %bitcast.9, f32[1,2048]{1,0:T(1,128)} %bitcast.8, s32[2,128]{1,0:T(2,128)} %bitcast.10, ...), custom_call_target="tpu_custom_call" | custom-call | tf_op jit(solution)/shard_map/pallas_call | solution.py:422
  77.2 1.9 %copy.17 = bf16[128,2048]{1,0:T(8,128)(2,1)} copy(bf16[128,2048]{1,0:T(8,128)(2,1)} %shard_map.145) | data formatting | bytes 1048576

commit v5 on v4

--- a/solution.py
+++ b/solution.py
@@ -13,9 +13,9 @@
 MESH = pl.DeviceIdType.MESH
 SEG = 8
 STEPS = 32
-CHUNKS = 4
-PER_CHUNK = 16
-EARLY = 1
+PER_CHUNK = 8
+CHUNKS = 64 // PER_CHUNK
+EARLY = 3
 EARLY_SLOTS = EARLY * PER_CHUNK
 
 
@@ -31,9 +31,13 @@
     total, order = [0.0] * 6, [(0, 0, 0)]
     while left:
 
+        near = len(order) < EARLY_SLOTS
+        limit = 2 if near else 6
+
         def cost(shift):
+            hops = sum(steps_of(shift))
             now = [a + b for a, b in zip(total, steps_of(shift))]
-            return (max(now) - min(now), -sum(steps_of(shift)))
+            return (hops > limit, max(now) - min(now), hops if near else -hops)
 
         best = min(left, key=cost)
         left.remove(best)
@@ -312,7 +316,7 @@
     pre_copy = remote(pre.at[k], pre.at[k], psend.at[2], precv.at[2], (c, other))
     pre_copy.start()
 
-    send_rows(1, 16)
+    send_rows(1, EARLY_SLOTS)
 
     loads[0].wait()
     lin = dot(pre[k], glu[pl.ds(pl.multiple_of(k * 512, 512), 512), :])
@@ -378,27 +382,40 @@
         if q == 0:
             ret[0] = ans[0]
 
-    for half in range(2):
-        for q in range(half * CHUNKS // 2, (half + 1) * CHUNKS // 2):
-            arrived(ret, bsem, q).wait_recv()
-        returned = ret[32 * half : 32 * half + 32].reshape(256, 2048)
-        high = slice(256 * half, 256 * half + 256)
-        low = slice(512 + 256 * half, 768 + 256 * half)
-        theirs, mine = comb[other], comb[k]
-        routed = dot(theirs[:, high], returned) + dot(theirs[:, low], returned)
-        if half == 0:
-            part_sum[...] = routed
-            own_rows = pl.ds(pl.multiple_of(k * 128, 128), 128)
-            own_sum[...] = (
-                mixed[own_rows, :] + dot(mine[:, high], returned) + dot(mine[:, low], returned)
-            )
-        else:
-            part_out[...] = (part_sum[...] + routed).astype(BF16)
-            part_copy = remote(part_out, part_in, psend.at[3], precv.at[3], (c, other))
-            part_copy.start()
-            own_sum[...] = own_sum[...] + dot(mine[:, high], returned) + dot(mine[:, low], returned)
-    part_copy.wait()
-    o_ref[...] = (own_sum[...] + part_in[...].astype(F32)).astype(BF16)
+    for q in range(CHUNKS - 1):
+        arrived(ret, bsem, q).wait_recv()
+    last = 512 - 8 * PER_CHUNK
+    theirs, mine = comb[other], comb[k]
+    returned = ret[0 : 64 - PER_CHUNK].reshape(last, 2048)
+    own_rows = pl.ds(pl.multiple_of(k * 128, 128), 128)
+    part_sum[...] = dot(theirs[:, 0:last], returned) + dot(theirs[:, 512 : 512 + last], returned)
+    own_sum[...] = (
+        mixed[own_rows, :]
+        + dot(mine[:, 0:last], returned)
+        + dot(mine[:, 512 : 512 + last], returned)
+    )
+    theirs = jnp.concatenate([theirs[:, last:512], theirs[:, 512 + last : 1024]], axis=1)
+    mine = jnp.concatenate([mine[:, last:512], mine[:, 512 + last : 1024]], axis=1)
+    arrived(ret, bsem, CHUNKS - 1).wait_recv()
+    pieces = []
+    for n in range(4):
+        cols = slice(512 * n, 512 * n + 512)
+        tail = ret[64 - PER_CHUNK : 64, :, cols].reshape(8 * PER_CHUNK, 512)
+        tail = jnp.concatenate([tail, tail], axis=0)
+        part_out[n] = (part_sum[:, cols] + dot(theirs, tail)).astype(BF16)
+        pieces.append(
+            remote(part_out.at[n], part_in.at[n], psend.at[5 + n], precv.at[5 + n], (c, other))
+        )
+        pieces[n].start()
+    for n in range(4):
+        cols = slice(512 * n, 512 * n + 512)
+        tail = ret[64 - PER_CHUNK : 64, :, cols].reshape(8 * PER_CHUNK, 512)
+        tail = jnp.concatenate([tail, tail], axis=0)
+        own_sum[:, cols] = own_sum[:, cols] + dot(mine, tail)
+    for n in range(4):
+        cols = slice(512 * n, 512 * n + 512)
+        pieces[n].wait()
+        o_ref[:, cols] = (own_sum[:, cols] + part_in[n].astype(F32)).astype(BF16)
 
     def line_sent(target, carry):
         remote(line, ybuf.at[ln], ys.at[target], yr.at[ln], (target * 4 + x, k)).wait_send()
@@ -450,14 +467,14 @@
             pltpu.VMEM((64, 8, 2048), BF16),
             pltpu.VMEM((64, 8, 2048), BF16),
             pltpu.VMEM((64, 8, 2048), BF16),
-            pltpu.VMEM((128, 2048), BF16),
-            pltpu.VMEM((128, 2048), BF16),
+            pltpu.VMEM((4, 128, 512), BF16),
+            pltpu.VMEM((4, 128, 512), BF16),
             pltpu.VMEM((128, 2048), F32),
             pltpu.VMEM((128, 2048), F32),
             pltpu.VMEM((EARLY_SLOTS, 8, 1024), BF16),
             pltpu.VMEM((EARLY_SLOTS, 8, 1024), BF16),
-            dma((6,)), dma((3,)), dma((3,)), dma((16,)), dma((16,)), dma((5,)), dma((5,)),
-            dma((4,)), dma((4,)), dma((4,)), dma((4,)), dma((EARLY,)), dma((EARLY,)),
+            dma((6,)), dma((3,)), dma((3,)), dma((16,)), dma((16,)), dma((9,)), dma((9,)),
+            dma((CHUNKS,)), dma((CHUNKS,)), dma((CHUNKS,)), dma((CHUNKS,)), dma((EARLY,)), dma((EARLY,)),
         ],
         compiler_params=pltpu.CompilerParams(
             collective_id=0, has_side_effects=True, vmem_limit_bytes=60 * 1024 * 1024

time: 79.3 us -> 78.8 us (level)
  no operation moved by 1% of the time
where the time goes in v5:
time: 78.8 us; the launch traced here: 78.6 us
  Pallas kernels  76.7 us (97%)
  local copies, waits for them, and re-layouts  1.88 us (2%)
    pallas_call x1, Pallas kernels, on_device(): pl.pallas_call(body, out_shape=jax.ShapeDtypeStruct((128, 2048), BF16), i...  76.7 us
    unnamed x1, local copies, waits for them, and re-layouts  1.88 us

profile of v5, /device:TPU:1, one launch (start us, length us, event | category | flops | bytes accessed | tf_op | source)
XLA Modules:
  0.0 78.6 jit_solution(6550836984729074751)
XLA Ops:
  0.0 76.7 %shard_map.145 = bf16[128,2048]{1,0:T(8,128)(2,1)} custom-call(bf16[256,512]{1,0:T(8,128)(2,1)} %u_ref.1, f32[32,64]{1,0:T(8,128)} %lr_ref.1, f32[32,64]{1,0:T(8,128)} %li_ref.1, f32[2,512,64]{2,1,0:T(8,128)} %bitcast.6, f32[32,16,128]{2,1,0:T(8,128)} %bitcast.7, f32[1,512]{1,0:T(1,128)} %bitcast.9, f32[1,2048]{1,0:T(1,128)} %bitcast.8, s32[2,128]{1,0:T(2,128)} %bitcast.10, ...), custom_call_target="tpu_custom_call" | custom-call | tf_op jit(solution)/shard_map/pallas_call | solution.py:439
  76.7 1.9 %copy.17 = bf16[128,2048]{1,0:T(8,128)(2,1)} copy(bf16[128,2048]{1,0:T(8,128)(2,1)} %shard_map.145) | data formatting | bytes 1048576
